TPU v7x, 512 devices: a whole 4x4x16 slice. The times are simulated.
512 devices in a mesh: fs: 64 (over z, y), tp: 8 (over x, core).
Axes of the slice: x: 4, y: 4, z: 16, core: 2. Of those that a mesh axis runs over, the one named last changes fastest.
Arguments:
- saved_inputs: bfloat16 [49152, 2048], P('fs'), may hold values from -16 to 16
- input_cot: bfloat16 [49152, 2048], P('fs', 'tp'), may hold values from -0.02734375 to 0.02734375
- gate_cot: bfloat16 [49152, 2048], P('fs', 'tp'), may hold values from -0.02734375 to 0.02734375
- input_master: float32 [2048, 2048], P('fs', 'tp'), may hold values from -6 to 6
- gate_master: float32 [2048, 2048], P('fs', 'tp'), may hold values from -6 to 6
- input_factor: bfloat16 [2048, 256], P('fs'), may hold values from -2 to 2
- gate_factor: bfloat16 [2048, 256], P('fs'), may hold values from -2 to 2
- input_first: float32 [256, 2048], P('fs', 'tp'), may hold values from -6 to 6
- input_second: float32 [256, 2048], P('fs', 'tp'), may hold values from 0.2 to 17
- gate_first: float32 [256, 2048], P('fs', 'tp'), may hold values from -6 to 6
- gate_second: float32 [256, 2048], P('fs', 'tp'), may hold values from 0.2 to 17
Outputs:
- input_step: float32 [2048, 2048], P('fs', 'tp')
- gate_step: float32 [2048, 2048], P('fs', 'tp')
- input_first_new: float32 [256, 2048], P('fs', 'tp')
- input_second_new: float32 [256, 2048], P('fs', 'tp')
- gate_first_new: float32 [256, 2048], P('fs', 'tp')
- gate_second_new: float32 [256, 2048], P('fs', 'tp')
- input_copy: bfloat16 [2048, 2048], P(None, 'tp')
- gate_copy: bfloat16 [2048, 2048], P(None, 'tp')
All inputs are finite; a program needn't handle non-finite values.
Results may differ from a plain program's by a relative error of at most 0.0004.
Values may be sent and summed in bfloat16 or wider, within the bound.
A program may use at most 64 MiB of HBM per device.

v0:
```python
import jax
import jax.numpy as jnp
from jax import lax
from jax.sharding import Mesh
from jax.sharding import PartitionSpec as P

D = 2048
W = 2048
FS = ("fs_0", "fs_1")
FS_TP = ("fs_0", "fs_1", "tp_0", "tp_1")
TP = ("tp_0", "tp_1")


first_decay = 0.9
second_decay = 0.9
ratio_floor = 1e-08
mean_floor = 1e-06
step_size = 0.05


def own_block(parts, axes, order):
    shape = [lax.axis_size(a) for a in axes]
    parts = parts.reshape(*shape, *parts.shape[1:])
    parts = parts.transpose(*order, *range(len(axes), parts.ndim))
    parts = parts.reshape(-1, *parts.shape[len(axes) :])
    for k in order:
        parts = lax.psum_scatter(parts, axes[k], scatter_dimension=0, tiled=True)
    return parts[0]


def split_up(shard, dim, count):
    before, after = (shard.shape[:dim], shard.shape[dim + 1 :])
    return jnp.moveaxis(shard.reshape(*before, count, -1, *after), dim, 0)


def summed_rows(shard, axes, order, dim):
    count = lax.axis_size(axes)
    return own_block(split_up(shard, dim, count), axes, order)


def sent_and_summed(shard, axis, dim):
    count = lax.axis_size(axis)
    parts = lax.all_to_all(split_up(shard, dim, count), axis, 0, 0, tiled=True)
    return jnp.sum(parts, axis=0)


def sent_together(arrays, axis, dim, along):
    widths = [a.shape[along] for a in arrays]
    both = jnp.concatenate(arrays, axis=along)
    out = sent_and_summed(both, axis, dim)
    return tuple(jnp.split(out, [sum(widths[:k]) for k in range(1, len(widths))], axis=along))


def in_one_piece(arrays, axis, dim, along):
    both = jnp.concatenate(arrays, axis=along)
    out, at, finished = (lax.all_gather(both, axis, axis=dim, tiled=True), 0, [])
    for a in arrays:
        finished.append(lax.slice_in_dim(out, at, at + a.shape[along], axis=along))
        at += a.shape[along]
    return tuple(finished)


def one_axis_at_a_time(shard, axes):
    for axis in axes:
        shard = lax.psum(shard, axis)
    return shard


def moments(low_rank, first, second):
    first_new = first_decay * first + (1.0 - first_decay) * low_rank
    second_new = second_decay * second + (1.0 - second_decay) * low_rank * low_rank
    ratio = first_new / (jnp.sqrt(second_new) + ratio_floor)
    return (first_new, second_new, ratio)


def local(
    saved_inputs,
    input_cot,
    gate_cot,
    input_master,
    gate_master,
    input_factor,
    gate_factor,
    input_first,
    input_second,
    gate_first,
    gate_second,
):
    col_width = input_cot.shape[1]
    contract = (((0,), (0,)), ((), ()))
    factor_in = input_factor.astype(jnp.float32)
    factor_gate = gate_factor.astype(jnp.float32)
    term_in = lax.dot_general(saved_inputs, input_cot, contract, preferred_element_type=jnp.float32)
    term_gate = lax.dot_general(
        saved_inputs, gate_cot, contract, preferred_element_type=jnp.float32
    )
    gradients = summed_rows(jnp.concatenate([term_in, term_gate], axis=1), FS, (1, 0), 0)
    part_in = lax.dot_general(
        factor_in, gradients[:, :col_width], contract, precision=lax.Precision.HIGHEST
    )
    part_gate = lax.dot_general(
        factor_gate, gradients[:, col_width:], contract, precision=lax.Precision.HIGHEST
    )
    low_in, low_gate = sent_together((part_in, part_gate), FS, 0, 1)
    first_in, second_in, ratio_in = moments(low_in, input_first, input_second)
    first_gate, second_gate, ratio_gate = moments(low_gate, gate_first, gate_second)
    piece_in, piece_gate = in_one_piece((ratio_in, ratio_gate), FS, 0, 1)
    dir_in = jnp.dot(factor_in, piece_in, precision=lax.Precision.HIGHEST)
    dir_gate = jnp.dot(factor_gate, piece_gate, precision=lax.Precision.HIGHEST)
    square_in, square_gate = (
        one_axis_at_a_time(jnp.sum(dir_in * dir_in), FS_TP),
        one_axis_at_a_time(jnp.sum(dir_gate * dir_gate), FS_TP),
    )
    step_in = dir_in * lax.rsqrt(square_in / (D * W) + mean_floor)
    step_gate = dir_gate * lax.rsqrt(square_gate / (D * W) + mean_floor)
    local_in = (input_master - step_size * step_in).astype(jnp.bfloat16)
    local_gate = (gate_master - step_size * step_gate).astype(jnp.bfloat16)
    copy_in, copy_gate = in_one_piece((local_in, local_gate), FS, 0, 1)
    return (step_in, step_gate, first_in, second_in, first_gate, second_gate, copy_in, copy_gate)


def solution(mesh):
    finer = Mesh(mesh.devices.reshape(16, 4, 4, 2), ("fs_0", "fs_1", "tp_0", "tp_1"))
    placed = (
        P(FS, None),
        P(FS, TP),
        P(FS, TP),
        P(FS, TP),
        P(FS, TP),
        P(FS, None),
        P(FS, None),
        P(FS, TP),
        P(FS, TP),
        P(FS, TP),
        P(FS, TP),
    )
    return jax.shard_map(
        local,
        mesh=finer,
        in_specs=placed,
        out_specs=(
            P(FS, TP),
            P(FS, TP),
            P(FS, TP),
            P(FS, TP),
            P(FS, TP),
            P(FS, TP),
            P(None, TP),
            P(None, TP),
        ),
        check_vma=False,
    )
```

profile of v0, /device:TPU:1, one launch (start us, length us, event | category | flops | bytes accessed | tf_op | source)
XLA Modules:
  0.0 501.9 jit_solution(1282623223704920424)
XLA Ops:
  7.2 0.0 copy-start
  7.2 0.0 copy-start.1
  7.2 0.0 reduce-scatter.3.cloned.1.call-start
  7.2 1.8 copy-done
  9.1 2.0 fusion.11
  11.1 0.0 copy-done.1
  11.1 1.0 fusion.12
  12.1 2.5 pad_maximum_fusion
  14.6 5.3 %copy.22 = f32[2048,512]{1,0:T(8,128)} copy(f32[2048,512]{0,1:T(8,128)} %pad_maximum_fusion) | data formatting | bytes 8388608 | tf_op jit(solution)/shard_map/concatenate | solution.py:97
  19.9 5.0 copy.23
  24.9 0.0 copy-start.2
  24.9 0.0 copy-start.3
  24.9 0.0 reduce-scatter.3.cloned.1.call-update
  24.9 0.0 reduce-scatter.5.cloned.1.call-start
  25.0 59.9 %reduce-scatter.3.cloned.1.call-done = f32[16,32,512]{2,1,0:T(8,128)} async-done(((f32[64,32,512]{2,1,0:T(8,128)}), f32[16,32,512]{2,1,0:T(8,128)}) %reduce-scatter.3.cloned.1.call-update) | async-done | bytes 1048592 | tf_op jit(solution)/shard_map/reduce_scatter | solution.py:27
  84.8 0.0 copy-start.6
  84.8 0.0 copy-start.7
  84.8 0.0 copy-start.8
  84.8 0.0 copy-start.9
  84.8 0.0 reduce-scatter.5.cloned.1.call-update
  84.9 0.0 all-gather.3.cloned.1.call-start
  84.9 63.5 %reduce-scatter.5.cloned.1.call-done = f32[1,32,512]{2,1,0:T(8,128)} async-done(((f32[16,32,512]{2,1,0:T(8,128)}), f32[1,32,512]{2,1,0:T(8,128)}) %reduce-scatter.5.cloned.1.call-update) | async-done | bytes 65552 | tf_op jit(solution)/shard_map/reduce_scatter | solution.py:27
  148.5 0.0 copy-done.2
  148.5 1.1 convolution_bitcast_fusion
  149.5 0.0 copy-done.3
  149.6 1.1 convolution_bitcast_fusion.1
  150.6 0.8 pad_maximum_fusion.1
  151.5 0.0 copy-start.4
  151.5 0.0 copy-start.5
  151.5 2.0 copy.24
  153.5 2.0 reshape.23
  155.5 33.6 %all_to_all.5 = f32[64,4,512]{2,1,0:T(4,128)} all-to-all(f32[64,4,512]{2,1,0:T(4,128)} %reshape.23), channel_id=1, replica_groups=mesh['fs_0'=16,'fs_1'=4,'tp_0'=4,'tp_1'=2] {'fs_0','fs_1'}, dimensions={0} | all-to-all | bytes 1048576 | tf_op jit(solution)/shard_map/all_to_all | solution.py:43
  189.1 1.2 reduce_sum.27
  190.2 0.0 copy-done.6
  190.2 0.0 copy-done.7
  190.2 0.0 copy-done.8
  190.2 0.0 copy-done.9
  190.3 0.6 add_divide_fusion.1
  190.9 82.0 %all-gather = f32[64,4,512]{2,1,0:T(4,128)} all-gather(f32[1,4,512]{2,1,0:T(4,128)S(1)} %maximum_bitcast_fusion), channel_id=1, replica_groups=mesh['fs_0'=16,'fs_1'=4,'tp_0'=4,'tp_1'=2] {'fs_0','fs_1'}, dimensions={0}, use_global_device_ids=true | all-gather | bytes 532480 | tf_op jit(solution)/shard_map/all_gather | solution.py:56
  272.8 2.0 reshape.25
  274.9 1.8 multiply_reduce_fusion
  276.6 1.8 multiply_reduce_fusion.1
  278.4 23.2 %all-reduce = (f32[]{:T(128)}, f32[]{:T(128)}) all-reduce(f32[]{:T(128)} %get-tuple-element.31, f32[]{:T(128)} %get-tuple-element.33), channel_id=1, replica_groups=mesh['fs_0'=16,'fs_1'=4,'tp_0'=4,'tp_1'=2] {'fs_0'}, use_global_device_ids=true, to_apply=%region_4.0 | all-reduce | flops 2 | bytes 16 | tf_op jit(solution)/shard_map/psum | solution.py:65
  301.6 7.1 %all-reduce.2 = (f32[]{:T(128)}, f32[]{:T(128)}) all-reduce(f32[]{:T(128)} %get-tuple-element.8, f32[]{:T(128)} %get-tuple-element.9), channel_id=1, replica_groups=mesh['fs_0'=16,'fs_1'=4,'tp_0'=4,'tp_1'=2] {'fs_1'}, use_global_device_ids=true, to_apply=%region_5.0 | all-reduce | flops 2 | bytes 16 | tf_op jit(solution)/shard_map/psum | solution.py:65
  308.7 9.0 %all-reduce.1 = (f32[]{:T(128)}, f32[]{:T(128)}) all-reduce(f32[]{:T(128)} %get-tuple-element.12, f32[]{:T(128)} %get-tuple-element.13), channel_id=1, replica_groups=mesh['fs_0'=16,'fs_1'=4,'tp_0'=4,'tp_1'=2] {'tp_0'}, use_global_device_ids=true, to_apply=%region_6.0 | all-reduce | flops 2 | bytes 16 | tf_op jit(solution)/shard_map/psum | solution.py:65
  317.7 51.9 %all-reduce.3 = (f32[]{:T(128)}, f32[]{:T(128)}) all-reduce(f32[]{:T(128)} %get-tuple-element.10, f32[]{:T(128)} %get-tuple-element.11), channel_id=1, replica_groups=mesh['fs_0'=16,'fs_1'=4,'tp_0'=4,'tp_1'=2] {'tp_1'}, use_global_device_ids=true, to_apply=%region_7.0 | all-reduce | flops 2 | bytes 16 | tf_op jit(solution)/shard_map/psum | solution.py:65
  370.9 0.0 copy-done.4
  371.0 0.0 copy-done.5
  371.0 0.6 subtract_convert_fusion
  371.6 0.6 pad_maximum_fusion.2
  372.2 0.0 all-gather.3.cloned.1.call-update
  372.2 120.1 %all-gather.3.cloned.1.call-done = bf16[2048,512]{1,0:T(8,128)(2,1)} async-done(((bf16[32,512]{1,0:T(8,128)(2,1)}), bf16[2048,512]{1,0:T(8,128)(2,1)}) %all-gather.3.cloned.1.call-update) | async-done | bytes 2097168 | tf_op jit(solution)/shard_map/all_gather | solution.py:56
  492.4 3.0 fusion.10
  (1 shorter events, 0.0 us)
Async XLA Ops:
  7.2 1.9 copy-start
  7.2 3.9 copy-start.1
  7.2 77.6 %reduce-scatter.3.cloned.1.call-start = ((), (), s32[]{:S(2)}) async-start(), calls=%async_computation.3 | async-start | bytes 5242880 | tf_op jit(solution)/shard_map/reduce_scatter | solution.py:27
  24.9 123.6 %copy-start.2 = (bf16[32,256]{1,0:T(8,128)(2,1)S(1)}, bf16[32,256]{1,0:T(8,128)(2,1)}, u32[]{:S(2)}) copy-start(bf16[32,256]{1,0:T(8,128)(2,1)} %param.17) | copy-start | bytes 49156
  24.9 124.7 %copy-start.3 = (bf16[32,256]{1,0:T(8,128)(2,1)S(1)}, bf16[32,256]{1,0:T(8,128)(2,1)}, u32[]{:S(2)}) copy-start(bf16[32,256]{1,0:T(8,128)(2,1)} %param.16) | copy-start | bytes 49156
  24.9 123.6 %reduce-scatter.5.cloned.1.call-start = ((), (), s32[]{:S(2)}) async-start(), calls=%async_computation.4 | async-start | bytes 1114112 | tf_op jit(solution)/shard_map/reduce_scatter | solution.py:27
  84.8 105.4 %copy-start.6 = (f32[4,256]{1,0:T(4,128)S(1)}, f32[4,256]{1,0:T(4,128)}, u32[]{:S(2)}) copy-start(f32[4,256]{1,0:T(4,128)} %param.19) | copy-start | bytes 12292
  84.8 105.4 %copy-start.7 = (f32[4,256]{1,0:T(4,128)S(1)}, f32[4,256]{1,0:T(4,128)}, u32[]{:S(2)}) copy-start(f32[4,256]{1,0:T(4,128)} %param.18) | copy-start | bytes 12292
  84.8 105.4 %copy-start.8 = (f32[4,256]{1,0:T(4,128)S(1)}, f32[4,256]{1,0:T(4,128)}, u32[]{:S(2)}) copy-start(f32[4,256]{1,0:T(4,128)} %param.21) | copy-start | bytes 12292
  84.8 105.4 %copy-start.9 = (f32[4,256]{1,0:T(4,128)S(1)}, f32[4,256]{1,0:T(4,128)}, u32[]{:S(2)}) copy-start(f32[4,256]{1,0:T(4,128)} %param.20) | copy-start | bytes 12292
  84.9 407.5 %all-gather.3.cloned.1.call-start = ((), (), s32[]{:S(2)}) async-start(), calls=%async_computation.5 | async-start | bytes 2129920 | tf_op jit(solution)/shard_map/all_gather | solution.py:56
  151.5 219.5 %copy-start.4 = (f32[32,256]{1,0:T(8,128)S(1)}, f32[32,256]{1,0:T(8,128)}, u32[]{:S(2)}) copy-start(f32[32,256]{1,0:T(8,128)} %param.15) | copy-start | bytes 98308
  151.5 219.5 %copy-start.5 = (f32[32,256]{1,0:T(8,128)S(1)}, f32[32,256]{1,0:T(8,128)}, u32[]{:S(2)}) copy-start(f32[32,256]{1,0:T(8,128)} %param.14) | copy-start | bytes 98308
Sparse Core Ops, SparseCore 0:
  25.0 59.7 reduce-scatter.2
  87.6 60.7 reduce-scatter.4
  372.4 119.9 all-gather.2
where the time goes:
time: 512 us; the launch traced here: 502 us
  waiting for transfers between devices  244 us (48%)
  blocking collectives  207 us (40%)
  local copies, waits for them, and re-layouts  21.2 us (4%)
  between operations  15.2 us (3%)
  matrix products  8.73 us (2%)
  other arithmetic  6.31 us (1%)
    reduce_scatter x2, waiting for transfers between devices, own_block(): parts = lax.psum_scatter(parts, axes[k], scatter_dimension=0, tiled=True)  123 us
    all_gather x1, waiting for transfers between devices, in_one_piece(): lax.all_gather(both, axis, axis=dim, tiled=True)  120 us
    psum x4, blocking collectives, one_axis_at_a_time(): shard = lax.psum(shard, axis)  91.2 us
    all_gather x1, blocking collectives, in_one_piece(): lax.all_gather(both, axis, axis=dim, tiled=True)  82 us
    all_to_all x1, blocking collectives, sent_and_summed(): parts = lax.all_to_all(split_up(shard, dim, count), axis, 0, 0, tiled=True)  33.6 us
  transfers between devices with their start and end apart: 3, of which 3 were waited for; matrix products, arithmetic and copies ran while one was open for 0% of the time, Pallas kernels for 0%

commit v1 on v0

v1 whole, which is shorter than its diff:
```python
import functools

import jax
import jax.numpy as jnp
from jax import lax
from jax.experimental import pallas as pl
from jax.experimental.pallas import tpu as pltpu
from jax.sharding import Mesh
from jax.sharding import PartitionSpec as P

D = 2048
W = 2048
FS = ("fs_0", "fs_1")
TP = ("tp_0", "tp_1")
NZ, NY, NX, NC = 16, 4, 4, 2
HALF = NZ // 2

first_decay = 0.9
second_decay = 0.9
ratio_floor = 1e-08
mean_floor = 1e-06
step_size = 0.05

f32 = jnp.float32
bf16 = jnp.bfloat16


def remote(src, dst, send_sem, recv_sem, **where):
    return pltpu.make_async_remote_copy(
        src_ref=src,
        dst_ref=dst,
        send_sem=send_sem,
        recv_sem=recv_sem,
        device_id=where,
        device_id_type=pl.DeviceIdType.MESH,
    )


def split_two(v):
    high = v.astype(bf16)
    low = (v - high.astype(f32)).astype(bf16)
    return high, low


def kernel(
    x_hbm, cin_hbm, cg_hbm, min_hbm, mg_hbm, fin_hbm, fg_hbm, a1, a2, g1, g2,
    step_in, step_g, o_a1, o_a2, o_g1, o_g2, copy_in, copy_g,
    xb, cb, mb, fb, lowb, rsy, l2, rsz, rb, dirb, sb, cpy,
    loc_sem, fz_s, fz_r, f1_s, f1_r, f2_s, f2_r, fc_s, fc_r,
    ry_s, ry_r, rz_s, rz_r, gz_s, gz_r, gy_s, gy_r, sc_s, sc_r,
    cz_s, cz_r, cy_s, cy_r, out_sem,
):
    z = lax.axis_index("fs_0")
    y = lax.axis_index("fs_1")
    x = lax.axis_index("tp_0")
    c = lax.axis_index("tp_1")
    other = 1 - c

    def zz(k):
        return lax.rem(z + k + NZ, NZ)

    def yy(k):
        return lax.rem(y + k + NY, NY)

    def xx(k):
        return lax.rem(x + k + NX, NX)

    barrier = pltpu.get_barrier_semaphore()

    def greet(k, _):
        pl.semaphore_signal(barrier, inc=1, device_id={"fs_0": zz(k)}, device_id_type=pl.DeviceIdType.MESH)
        return 0

    lax.fori_loop(1, NZ, greet, 0)
    for k in range(1, NY):
        pl.semaphore_signal(barrier, inc=1, device_id={"fs_1": yy(k)}, device_id_type=pl.DeviceIdType.MESH)
    tp_peers = [(dx, dc) for dx in range(NX) for dc in range(NC) if (dx, dc) != (0, 0)]
    for dx, dc in tp_peers:
        pl.semaphore_signal(
            barrier, inc=1,
            device_id={"tp_0": xx(dx), "tp_1": other if dc else c},
            device_id_type=pl.DeviceIdType.MESH,
        )

    h = x // 2
    tile = pl.ds(pl.multiple_of((c * 2 + lax.rem(x, 2)) * 128, 128), 128)
    wide = pl.ds(pl.multiple_of(c * 256, 256), 256)
    piece = pl.ds(pl.multiple_of(lax.rem(x, 2) * 128, 128), 128)

    def own_tile(source):
        return pltpu.make_async_copy(source.at[h, :, piece], fb.at[z, y, h, :, tile], loc_sem.at[0])

    @pl.when(c == 0)
    def _():
        own_tile(fin_hbm).start()

    @pl.when(c == 1)
    def _():
        own_tile(fg_hbm).start()

    loads = [
        pltpu.make_async_copy(x_hbm, xb, loc_sem.at[1]),
        pltpu.make_async_copy(cin_hbm, cb.at[0], loc_sem.at[2]),
        pltpu.make_async_copy(cg_hbm, cb.at[1], loc_sem.at[3]),
        pltpu.make_async_copy(min_hbm, mb.at[0], loc_sem.at[4]),
        pltpu.make_async_copy(mg_hbm, mb.at[1], loc_sem.at[5]),
    ]
    for copy in loads:
        copy.start()
    own_tile(fin_hbm).wait()
    pl.semaphore_wait(barrier, NZ - 1 + NY - 1 + len(tp_peers))

    def fz(k):
        part = fb.at[z, y, h, :, tile]
        return remote(part, part, fz_s.at[k], fz_r.at[k], fs_0=zz(k))

    def start(make):
        def body(k, _):
            make(k).start()
            return 0
        return body

    def wait_recv(make):
        def body(k, _):
            make(k).wait_recv()
            return 0
        return body

    def wait_send(make):
        def body(k, _):
            make(k).wait_send()
            return 0
        return body

    lax.fori_loop(1, NZ, start(fz), 0)
    lax.fori_loop(1, NZ, wait_recv(fz), 0)

    def half_step(part_x, part_y, send, recv):
        copies = []
        for k in range(1, NX):
            copies.append(remote(part_x, part_x, send.at[0, k], recv.at[0, k], tp_0=xx(k)))
        for k in range(1, NY):
            copies.append(remote(part_y, part_y, send.at[1, k], recv.at[1, k], fs_1=yy(k)))
        for copy in copies:
            copy.start()
        return copies

    lo_z, hi_z = pl.ds(0, HALF), pl.ds(HALF, HALF)
    one = half_step(fb.at[lo_z, y, h, :, tile], fb.at[hi_z, y, h, :, tile], f1_s, f1_r)
    for copy in one:
        copy.wait_recv()
    two = half_step(fb.at[hi_z, :, h, :, tile], fb.at[lo_z, y, :, :, wide], f2_s, f2_r)
    for copy in two:
        copy.wait_recv()
    mine = fb.at[:, :, :, :, wide]
    swap = remote(mine, mine, fc_s, fc_r, tp_1=other)
    swap.start()
    for copy in loads[:3]:
        copy.wait()
    swap.wait_recv()

    lows = []
    for f in range(2):
        total = jnp.zeros((256, 256), f32)
        factor = fb[:, :, :, :, f * 256:(f + 1) * 256].reshape(D, 256)
        for t in range(3):
            rows = pl.ds(t * 256, 256)
            proj = jnp.dot(xb[rows, :], factor, preferred_element_type=f32)
            high, low = split_two(proj.T)
            cot = cb[f, rows, :]
            total = total + jnp.dot(high, cot, preferred_element_type=f32)
            total = total + jnp.dot(low, cot, preferred_element_type=f32)
        lows.append(total.reshape(32, 8, 256))
    top = lax.broadcasted_iota(jnp.int32, (32, 8, 256), 1) < 4
    low_a, low_b = lows
    even = jnp.where(top, low_a, pltpu.roll(low_b, 4, 1))
    odd = jnp.where(top, pltpu.roll(low_a, 4, 1), low_b)
    for k in range(2):
        lowb[:, 2 * k] = even.reshape(16, 2, 8, 256)[:, k]
        lowb[:, 2 * k + 1] = odd.reshape(16, 2, 8, 256)[:, k]

    ry = [
        remote(lowb.at[:, yy(k)], rsy.at[k - 1], ry_s.at[k], ry_r.at[k], fs_1=yy(k))
        for k in range(1, NY)
    ]
    for copy in ry:
        copy.start()
    acc = lowb[:, y]
    for k, copy in enumerate(ry):
        copy.wait_recv()
        acc = acc + rsy[k]
    l2[...] = acc

    def rz(k):
        return remote(l2.at[zz(k)], rsz.at[k], rz_s.at[k], rz_r.at[k], fs_0=zz(k))

    lax.fori_loop(1, NZ, start(rz), 0)

    def add_one(k, total):
        rz(k).wait_recv()
        return total + rsz[k]

    low = lax.fori_loop(1, NZ, add_one, l2[z])

    first = jnp.concatenate([a1[...], g1[...]], axis=0)
    second = jnp.concatenate([a2[...], g2[...]], axis=0)
    first_new = first_decay * first + (1.0 - first_decay) * low
    second_new = second_decay * second + (1.0 - second_decay) * low * low
    rb[z, y] = first_new / (jnp.sqrt(second_new) + ratio_floor)

    def gz(k):
        part = rb.at[z, y]
        return remote(part, part, gz_s.at[k], gz_r.at[k], fs_0=zz(k))

    lax.fori_loop(1, NZ, start(gz), 0)
    o_a1[...] = first_new[:4]
    o_g1[...] = first_new[4:]
    o_a2[...] = second_new[:4]
    o_g2[...] = second_new[4:]
    lax.fori_loop(1, NZ, wait_recv(gz), 0)
    gy = [
        remote(rb.at[:, y], rb.at[:, y], gy_s.at[k], gy_r.at[k], fs_1=yy(k))
        for k in range(1, NY)
    ]
    for copy in gy:
        copy.start()
    for copy in gy:
        copy.wait_recv()

    ratio = rb[...].reshape(32, 2, 8, 256)
    even, odd = ratio[:, 0], ratio[:, 1]
    pieces = (
        jnp.where(top, even, pltpu.roll(odd, 4, 1)).reshape(256, 256),
        jnp.where(top, pltpu.roll(even, 4, 1), odd).reshape(256, 256),
    )
    for f in range(2):
        high, lo = split_two(pieces[f])

        def rows_of(t, acc, f=f, high=high, lo=lo):
            block = fb[pl.ds(t * 2, 2), :, :, :, f * 256:(f + 1) * 256].reshape(256, 256)
            d = jnp.dot(block, high, preferred_element_type=f32)
            d = d + jnp.dot(block, lo, preferred_element_type=f32)
            dirb[f, pl.ds(pl.multiple_of(t * 256, 256), 256), :] = d
            return acc + jnp.sum((d * d).reshape(32, 8, 256), axis=0)

        acc = lax.fori_loop(0, 8, rows_of, jnp.zeros((8, 256), f32))
        sb[0, f] = acc[:, :128] + acc[:, 128:]

    sc = [
        remote(
            sb.at[0], sb.at[k + 1], sc_s.at[k], sc_r.at[k],
            tp_0=xx(dx), tp_1=other if dc else c,
        )
        for k, (dx, dc) in enumerate(tp_peers)
    ]
    for copy in sc:
        copy.start()
    for copy in loads[3:]:
        copy.wait()
    for copy in sc:
        copy.wait_recv()
    own = pl.ds(pl.multiple_of((z * NY + y) * 32, 32), 32)
    for f, out in enumerate((step_in, step_g)):
        total = jnp.sum(jnp.sum(sb[:, f], axis=0), keepdims=True)
        scale = lax.rsqrt(total / (D * W) + mean_floor)
        step = dirb[f, own, :] * scale
        out[...] = step
        cpy[f, z, y] = (mb[f] - step_size * step).astype(bf16)

    both = pl.ds(0, 2)

    def cz(s, way, mats=both):
        block = cpy.at[mats, zz(1 - s) if way == 0 else zz(s - 1), y]
        return remote(block, block, cz_s.at[way, s], cz_r.at[way, s], fs_0=zz(1 if way == 0 else -1))

    def cy(o, way):
        block = cpy.at[:, zz(o), y]
        return remote(block, block, cy_s.at[way, o], cy_r.at[way, o], fs_1=yy(1 if way == 0 else -1))

    def on(o, way):
        mats = pl.ds(way, 1)
        block = cpy.at[mats, zz(o), yy(-1 if way == 0 else 1)]
        return remote(block, block, cy_s.at[way + 2, o], cy_r.at[way + 2, o], fs_1=yy(1 if way == 0 else -1))

    def send_y(o):
        cy(o, 0).start()
        cy(o, 1).start()

    def pass_y(o):
        cy(o, 0).wait_recv()
        on(o, 0).start()
        cy(o, 1).wait_recv()
        on(o, 1).start()

    cz(1, 0).start()
    cz(1, 1).start()
    send_y(0)

    def ring_one(s, _):
        cz(s, 0).wait_recv()
        cz(s + 1, 0).start()
        cz(s, 1).wait_recv()
        cz(s + 1, 1).start()
        send_y(s)
        send_y(NZ - s)
        return 0

    def ring(s, _):
        ring_one(s, 0)
        pass_y(s - 1)
        pass_y(NZ - s + 1)
        return 0

    ring_one(1, 0)
    pass_y(0)
    lax.fori_loop(2, HALF - 1, ring, 0)
    last = (cz(HALF, 0, pl.ds(0, 1)), cz(HALF, 1, pl.ds(1, 1)))
    for way in range(2):
        cz(HALF - 1, way).wait_recv()
        last[way].start()
    send_y(HALF - 1)
    send_y(HALF + 1)
    pass_y(HALF - 2)
    pass_y(HALF + 2)
    for way in range(2):
        last[way].wait_recv()
    send_y(HALF)
    pass_y(HALF - 1)
    pass_y(HALF + 1)
    pass_y(HALF)

    def finish(o, _):
        on(o, 0).wait_recv()
        on(o, 1).wait_recv()
        return 0

    lax.fori_loop(0, NZ, finish, 0)
    outs = [
        pltpu.make_async_copy(cpy.at[0], copy_in, out_sem.at[0]),
        pltpu.make_async_copy(cpy.at[1], copy_g, out_sem.at[1]),
    ]
    for copy in outs:
        copy.start()

    lax.fori_loop(1, NZ, wait_send(fz), 0)
    lax.fori_loop(1, NZ, wait_send(rz), 0)
    lax.fori_loop(1, NZ, wait_send(gz), 0)
    for copy in [*one, *two, swap, *ry, *gy, *sc, *last]:
        copy.wait_send()

    def drain_z(s, _):
        cz(s, 0).wait_send()
        cz(s, 1).wait_send()
        return 0

    def drain_y(o, _):
        for way in range(2):
            cy(o, way).wait_send()
            on(o, way).wait_send()
        return 0

    lax.fori_loop(1, HALF, drain_z, 0)
    lax.fori_loop(0, NZ, drain_y, 0)
    for copy in outs:
        copy.wait()


def local(x, cin, cg, m_in, m_g, f_in, f_g, a1, a2, g1, g2):
    vmem = pl.BlockSpec(memory_space=pltpu.VMEM)
    hbm = pl.BlockSpec(memory_space=pl.ANY)
    dma = pltpu.SemaphoreType.DMA
    out = pl.pallas_call(
        kernel,
        out_shape=(
            jax.ShapeDtypeStruct((32, 256), f32),
            jax.ShapeDtypeStruct((32, 256), f32),
            jax.ShapeDtypeStruct((4, 256), f32),
            jax.ShapeDtypeStruct((4, 256), f32),
            jax.ShapeDtypeStruct((4, 256), f32),
            jax.ShapeDtypeStruct((4, 256), f32),
            jax.ShapeDtypeStruct((NZ, NY, 32, 256), bf16),
            jax.ShapeDtypeStruct((NZ, NY, 32, 256), bf16),
        ),
        in_specs=[hbm] * 7 + [vmem] * 4,
        out_specs=(vmem,) * 6 + (hbm,) * 2,
        scratch_shapes=[
            pltpu.VMEM((768, 2048), bf16),
            pltpu.VMEM((2, 768, 256), bf16),
            pltpu.VMEM((2, 32, 256), f32),
            pltpu.VMEM((NZ, NY, 2, 16, 512), bf16),
            pltpu.VMEM((NZ, NY, 8, 256), f32),
            pltpu.VMEM((NY - 1, NZ, 8, 256), f32),
            pltpu.VMEM((NZ, 8, 256), f32),
            pltpu.VMEM((NZ, 8, 256), f32),
            pltpu.VMEM((NZ, NY, 8, 256), f32),
            pltpu.VMEM((2, 2048, 256), f32),
            pltpu.VMEM((NX * NC, 2, 8, 128), f32),
            pltpu.VMEM((2, NZ, NY, 32, 256), bf16),
            dma((6,)),
            dma((NZ,)), dma((NZ,)),
            dma((2, 4)), dma((2, 4)), dma((2, 4)), dma((2, 4)),
            dma, dma,
            dma((NY,)), dma((NY,)), dma((NZ,)), dma((NZ,)),
            dma((NZ,)), dma((NZ,)), dma((NY,)), dma((NY,)),
            dma((NX * NC,)), dma((NX * NC,)),
            dma((2, HALF + 1)), dma((2, HALF + 1)),
            dma((4, NZ)), dma((4, NZ)),
            dma((2,)),
        ],
        compiler_params=pltpu.CompilerParams(
            collective_id=0, has_side_effects=True, vmem_limit_bytes=48 * 1024 * 1024
        ),
    )(x, cin, cg, m_in, m_g, f_in.reshape(2, 16, 256), f_g.reshape(2, 16, 256), a1, a2, g1, g2)
    return (*out[:6], out[6].reshape(D, 256), out[7].reshape(D, 256))


def solution(mesh):
    finer = Mesh(mesh.devices.reshape(NZ, NY, NX, NC), ("fs_0", "fs_1", "tp_0", "tp_1"))
    rows, both = P(FS, None), P(FS, TP)
    return jax.shard_map(
        local,
        mesh=finer,
        in_specs=(rows, both, both, both, both, rows, rows, both, both, both, both),
        out_specs=(both,) * 6 + (P(None, TP),) * 2,
        check_vma=False,
    )
```

time: 512 us -> 137 us (0.27)
  the two profiles are of different devices: /device:TPU:1 before, /device:TPU:16 now
where the time goes in v1:
time: 137 us; the launch traced here: 136 us
  Pallas kernels  120 us (88%)
  local copies, waits for them, and re-layouts  15.1 us (11%)
    pallas_call x1, Pallas kernels, local(): pl.pallas_call(kernel, out_shape=(jax.ShapeDtypeStruct((32, 256), f32), j...  120 us
    unnamed x30, local copies, waits for them, and re-layouts  15.1 us

profile of v1, /device:TPU:16, one launch (start us, length us, event | category | flops | bytes accessed | tf_op | source)
XLA Modules:
  0.0 136.2 jit_solution(2794521671302934734)
XLA Ops:
  0.6 0.0 copy-start
  0.6 1.9 %copy-done = bf16[768,2048]{1,0:T(8,128)(2,1)S(1)} copy-done((bf16[768,2048]{1,0:T(8,128)(2,1)S(1)}, bf16[768,2048]{1,0:T(8,128)(2,1)}, u32[]{:S(2)}) %copy-start) | copy-done | bytes 3145752
  2.5 0.0 copy-start.1
  2.5 1.0 copy-done.1
  3.5 0.0 copy-start.2
  3.5 1.0 copy-done.2
  4.5 0.0 copy-start.3
  4.5 0.8 copy-done.3
  5.3 0.0 copy-start.4
  5.3 0.8 copy-done.4
  6.0 0.0 copy-start.5
  6.0 0.7 copy-done.5
  6.8 0.0 copy-start.6
  6.8 0.7 copy-done.6
  7.5 0.0 copy-start.7
  7.5 0.7 copy-done.7
  8.2 0.0 copy-start.8
  8.2 0.7 copy-done.8
  8.8 0.0 copy-start.9
  8.8 0.7 copy-done.9
  9.5 0.0 copy-start.10
  9.5 0.7 copy-done.10
  10.2 120.4 %shard_map.170 = (f32[32,256]{1,0:T(8,128)S(1)}, f32[32,256]{1,0:T(8,128)S(1)}, f32[4,256]{1,0:T(4,128)S(1)}, f32[4,256]{1,0:T(4,128)S(1)}, f32[4,256]{1,0:T(4,1...) custom-call(bf16[768,2048]{1,0:T(8,128)(2,1)S(1)} %copy-done, ...), custom_call_target="tpu_custom_call" | custom-call | tf_op jit(solution)/shard_map/pallas_call | solution.py:372
  130.6 0.6 copy.27
  131.3 0.6 copy.28
  131.9 0.6 copy.29
  132.5 0.6 copy.30
  133.1 0.6 copy.31
  133.6 0.6 copy.32
  134.2 1.0 copy.33
  135.2 1.0 copy.34
Async XLA Ops:
  0.6 1.9 %copy-start = (bf16[768,2048]{1,0:T(8,128)(2,1)S(1)}, bf16[768,2048]{1,0:T(8,128)(2,1)}, u32[]{:S(2)}) copy-start(bf16[768,2048]{1,0:T(8,128)(2,1)} %x_hbm.1) | copy-start | bytes 9437188
  2.5 1.0 copy-start.1
  3.5 1.0 copy-start.2
  4.5 0.8 copy-start.3
  5.3 0.8 copy-start.4
  6.0 0.7 copy-start.5
  6.8 0.7 copy-start.6
  7.5 0.7 copy-start.7
  8.2 0.7 copy-start.8
  8.8 0.7 copy-start.9
  9.5 0.7 copy-start.10

commit v2 on v1

v2 whole, which is shorter than its diff:
```python
import functools

import jax
import jax.numpy as jnp
from jax import lax
from jax.experimental import pallas as pl
from jax.experimental.pallas import tpu as pltpu
from jax.sharding import Mesh
from jax.sharding import PartitionSpec as P

D = 2048
W = 2048
FS = ("fs_0", "fs_1")
TP = ("tp_0", "tp_1")
NZ, NY, NX, NC = 16, 4, 4, 2
HALF = NZ // 2

first_decay = 0.9
second_decay = 0.9
ratio_floor = 1e-08
mean_floor = 1e-06
step_size = 0.05

f32 = jnp.float32
bf16 = jnp.bfloat16


def remote(src, dst, send_sem, recv_sem, **where):
    return pltpu.make_async_remote_copy(
        src_ref=src,
        dst_ref=dst,
        send_sem=send_sem,
        recv_sem=recv_sem,
        device_id=where,
        device_id_type=pl.DeviceIdType.MESH,
    )


def split_two(v):
    high = v.astype(bf16)
    low = (v - high.astype(f32)).astype(bf16)
    return high, low


def kernel(
    x_hbm, cin_hbm, cg_hbm, min_hbm, mg_hbm, fin_hbm, fg_hbm, a1_hbm, a2_hbm, g1_hbm, g2_hbm,
    step_in, step_g, o_a1, o_a2, o_g1, o_g2, copy_in, copy_g,
    xb, cb, mf, fb, mom, lowt, lowb, rsy, l2, rsz, rb, dirb, sb, cpy,
    loc_sem, fz_s, fz_r, f1_s, f1_r, f2_s, f2_r, fc_s, fc_r,
    ry_s, ry_r, rz_s, rz_r, gz_s, gz_r, gy_s, gy_r, sc_s, sc_r,
    za_s, za_r, zb_s, zb_r, ya_s, ya_r, yb_s, yb_r, out_sem,
):
    z = lax.axis_index("fs_0")
    y = lax.axis_index("fs_1")
    x = lax.axis_index("tp_0")
    c = lax.axis_index("tp_1")
    other = 1 - c

    def zz(k):
        return lax.rem(z + k + NZ, NZ)

    def yy(k):
        return lax.rem(y + k + NY, NY)

    def xx(k):
        return lax.rem(x + k + NX, NX)

    barrier = pltpu.get_barrier_semaphore()

    def greet(k, _):
        pl.semaphore_signal(barrier, inc=1, device_id={"fs_0": zz(k)}, device_id_type=pl.DeviceIdType.MESH)
        return 0

    lax.fori_loop(1, NZ, greet, 0)
    for k in range(1, NY):
        pl.semaphore_signal(barrier, inc=1, device_id={"fs_1": yy(k)}, device_id_type=pl.DeviceIdType.MESH)
    tp_peers = [(dx, dc) for dx in range(NX) for dc in range(NC) if (dx, dc) != (0, 0)]
    for dx, dc in tp_peers:
        pl.semaphore_signal(
            barrier, inc=1,
            device_id={"tp_0": xx(dx), "tp_1": other if dc else c},
            device_id_type=pl.DeviceIdType.MESH,
        )

    h = x // 2
    tile = pl.ds(pl.multiple_of((c * 2 + lax.rem(x, 2)) * 128, 128), 128)
    wide = pl.ds(pl.multiple_of(c * 256, 256), 256)
    piece = pl.ds(pl.multiple_of(lax.rem(x, 2) * 128, 128), 128)

    def own_tile(source):
        return pltpu.make_async_copy(source.at[h, :, piece], fb.at[z, y, h, :, tile], loc_sem.at[0])

    @pl.when(c == 0)
    def _():
        own_tile(fin_hbm).start()

    @pl.when(c == 1)
    def _():
        own_tile(fg_hbm).start()

    loads = [
        pltpu.make_async_copy(min_hbm, mf.at[0, z, y], loc_sem.at[1]),
        pltpu.make_async_copy(mg_hbm, mf.at[1, z, y], loc_sem.at[2]),
        pltpu.make_async_copy(x_hbm, xb, loc_sem.at[3]),
        pltpu.make_async_copy(cin_hbm, cb.at[0], loc_sem.at[4]),
        pltpu.make_async_copy(cg_hbm, cb.at[1], loc_sem.at[5]),
        pltpu.make_async_copy(a1_hbm, mom.at[0], loc_sem.at[6]),
        pltpu.make_async_copy(g1_hbm, mom.at[1], loc_sem.at[7]),
        pltpu.make_async_copy(a2_hbm, mom.at[2], loc_sem.at[8]),
        pltpu.make_async_copy(g2_hbm, mom.at[3], loc_sem.at[9]),
    ]
    for copy in loads:
        copy.start()
    own_tile(fin_hbm).wait()
    for copy in loads[:2]:
        copy.wait()
    pl.semaphore_wait(barrier, NZ - 1 + NY - 1 + len(tp_peers))

    def step_of(s, way):
        return (zz(1 - s), zz(1)) if way == 0 else (zz(s - 1), zz(-1))

    def za(s, way):
        at, to = step_of(s, way)
        part = mf.at[0, at, y, pl.ds(0, 32) if s < HALF else pl.ds(16 * way, 16)]
        return remote(part, part, za_s.at[way, s], za_r.at[way, s], fs_0=to)

    def zb(s, way):
        at, to = step_of(s, way)
        part = mf.at[1, at, pl.ds(0, 4) if s < HALF else pl.ds(2 * way, 2)]
        return remote(part, part, zb_s.at[way, s], zb_r.at[way, s], fs_0=to)

    def ring_start(make):
        for way in range(2):
            make(1, way).start()

    def ring_next(make, s):
        for way in range(2):
            make(s, way).wait_recv()
            if s < HALF:
                make(s + 1, way).start()

    def ya(o, way):
        part = mf.at[0, zz(o), y]
        return remote(part, part, ya_s.at[way, o], ya_r.at[way, o], fs_1=yy(1 if way == 0 else -1))

    def on(o, way):
        part = mf.at[0, zz(o), yy(-1 if way == 0 else 1), pl.ds(16 * way, 16)]
        return remote(part, part, ya_s.at[way + 2, o], ya_r.at[way + 2, o], fs_1=yy(1 if way == 0 else -1))

    def send_y(offsets):
        for o in offsets:
            for way in range(2):
                ya(o, way).start()

    def pass_y(offsets):
        for o in offsets:
            for way in range(2):
                ya(o, way).wait_recv()
                on(o, way).start()

    yb = [
        remote(mf.at[1, z, y], mf.at[1, z, y], yb_s.at[k], yb_r.at[k], fs_1=yy(k))
        for k in range(1, NY)
    ]

    def fz(k):
        part = fb.at[z, y, h, :, tile]
        return remote(part, part, fz_s.at[k], fz_r.at[k], fs_0=zz(k))

    def start(make):
        def body(k, _):
            make(k).start()
            return 0
        return body

    def wait_recv(make):
        def body(k, _):
            make(k).wait_recv()
            return 0
        return body

    def wait_send(make):
        def body(k, _):
            make(k).wait_send()
            return 0
        return body

    lax.fori_loop(1, NZ, start(fz), 0)
    ring_start(za)
    for copy in yb:
        copy.start()
    for copy in yb:
        copy.wait_recv()
    ring_start(zb)
    ring_next(za, 1)
    ring_next(za, 2)
    lax.fori_loop(1, NZ, wait_recv(fz), 0)

    def half_step(part_x, part_y, send, recv):
        copies = []
        for k in range(1, NX):
            copies.append(remote(part_x, part_x, send.at[0, k], recv.at[0, k], tp_0=xx(k)))
        for k in range(1, NY):
            copies.append(remote(part_y, part_y, send.at[1, k], recv.at[1, k], fs_1=yy(k)))
        for copy in copies:
            copy.start()
        return copies

    lo_z, hi_z = pl.ds(0, HALF), pl.ds(HALF, HALF)
    one = half_step(fb.at[lo_z, y, h, :, tile], fb.at[hi_z, y, h, :, tile], f1_s, f1_r)
    ring_next(zb, 1)
    for copy in one:
        copy.wait_recv()
    two = half_step(fb.at[hi_z, :, h, :, tile], fb.at[lo_z, y, :, :, wide], f2_s, f2_r)
    ring_next(za, 3)
    ring_next(zb, 2)
    for copy in two:
        copy.wait_recv()
    mine = fb.at[:, :, :, :, wide]
    swap = remote(mine, mine, fc_s, fc_r, tp_1=other)
    swap.start()
    ring_next(za, 4)
    for copy in loads[2:]:
        copy.wait()

    def project(f):
        total = jnp.zeros((256, 256), f32)
        factor = fb[:, :, :, :, pl.ds(pl.multiple_of(f * 256, 256), 256)].reshape(D, 256)
        for t in range(3):
            rows = pl.ds(t * 256, 256)
            proj = jnp.dot(xb[rows, :], factor, preferred_element_type=f32)
            high, low = split_two(proj.T)
            cot = cb[f, rows, :]
            total = total + jnp.dot(high, cot, preferred_element_type=f32)
            total = total + jnp.dot(low, cot, preferred_element_type=f32)
        lowt[f] = total.reshape(32, 8, 256)

    project(c)
    ring_next(zb, 3)
    ring_next(za, 5)
    swap.wait_recv()
    project(other)
    top = lax.broadcasted_iota(jnp.int32, (32, 8, 256), 1) < 4
    low_a, low_b = lowt[0], lowt[1]
    even = jnp.where(top, low_a, pltpu.roll(low_b, 4, 1))
    odd = jnp.where(top, pltpu.roll(low_a, 4, 1), low_b)
    for k in range(2):
        lowb[:, 2 * k] = even.reshape(16, 2, 8, 256)[:, k]
        lowb[:, 2 * k + 1] = odd.reshape(16, 2, 8, 256)[:, k]

    ry = [
        remote(lowb.at[:, yy(k)], rsy.at[k - 1], ry_s.at[k], ry_r.at[k], fs_1=yy(k))
        for k in range(1, NY)
    ]
    for copy in ry:
        copy.start()
    ring_next(zb, 4)
    ring_next(za, 6)
    acc = lowb[:, y]
    for k, copy in enumerate(ry):
        copy.wait_recv()
        acc = acc + rsy[k]
    l2[...] = acc

    def rz(k):
        return remote(l2.at[zz(k)], rsz.at[k], rz_s.at[k], rz_r.at[k], fs_0=zz(k))

    lax.fori_loop(1, NZ, start(rz), 0)
    early = [0, *(o for s in range(1, HALF - 1) for o in (s, NZ - s))]
    late = [HALF - 1, HALF + 1, HALF]
    send_y(early)
    ring_next(zb, 5)

    def add_one(k, total):
        rz(k).wait_recv()
        return total + rsz[k]

    low = lax.fori_loop(1, NZ, add_one, l2[z])

    first = jnp.concatenate([mom[0], mom[1]], axis=0)
    second = jnp.concatenate([mom[2], mom[3]], axis=0)
    first_new = first_decay * first + (1.0 - first_decay) * low
    second_new = second_decay * second + (1.0 - second_decay) * low * low
    rb[z, y] = first_new / (jnp.sqrt(second_new) + ratio_floor)

    def gz(k):
        part = rb.at[z, y]
        return remote(part, part, gz_s.at[k], gz_r.at[k], fs_0=zz(k))

    lax.fori_loop(1, NZ, start(gz), 0)
    o_a1[...] = first_new[:4]
    o_g1[...] = first_new[4:]
    o_a2[...] = second_new[:4]
    o_g2[...] = second_new[4:]
    pass_y(early)
    ring_next(zb, 6)
    lax.fori_loop(1, NZ, wait_recv(gz), 0)
    gy = [
        remote(rb.at[:, y], rb.at[:, y], gy_s.at[k], gy_r.at[k], fs_1=yy(k))
        for k in range(1, NY)
    ]
    for copy in gy:
        copy.start()
    ring_next(za, 7)
    ring_next(zb, 7)
    for copy in gy:
        copy.wait_recv()
    ring_next(za, HALF)
    send_y(late)

    ratio = rb[...].reshape(32, 2, 8, 256)
    even, odd = ratio[:, 0], ratio[:, 1]
    pieces = (
        jnp.where(top, even, pltpu.roll(odd, 4, 1)).reshape(256, 256),
        jnp.where(top, pltpu.roll(even, 4, 1), odd).reshape(256, 256),
    )
    for f in range(2):
        high, lo = split_two(pieces[f])

        acc = jnp.zeros((8, 256), f32)
        for t in range(4):
            block = fb[4 * t:4 * t + 4, :, :, :, f * 256:(f + 1) * 256].reshape(512, 256)
            d = jnp.dot(block, high, preferred_element_type=f32)
            d = d + jnp.dot(block, lo, preferred_element_type=f32)
            dirb[f, t] = d.reshape(16, 32, 256)
            acc = acc + jnp.sum((d * d).reshape(64, 8, 256), axis=0)
        sb[0, f] = acc[:, :128] + acc[:, 128:]

    sc = [
        remote(
            sb.at[0], sb.at[k + 1], sc_s.at[k], sc_r.at[k],
            tp_0=xx(dx), tp_1=other if dc else c,
        )
        for k, (dx, dc) in enumerate(tp_peers)
    ]
    for copy in sc:
        copy.start()
    pass_y(late)
    ring_next(zb, HALF)
    for o in [*early, *late]:
        for way in range(2):
            on(o, way).wait_recv()
    for copy in sc:
        copy.wait_recv()
    outs = []
    for f, (out, whole) in enumerate(((step_in, copy_in), (step_g, copy_g))):
        total = jnp.sum(jnp.sum(sb[:, f], axis=0), keepdims=True)
        scale = lax.rsqrt(total / (D * W) + mean_floor)
        for t in range(4):
            step = dirb[f, t] * scale.reshape(1, 1, 1)
            weights = mf[f, 4 * t:4 * t + 4].reshape(16, 32, 256)
            cpy[f, t] = (weights - step_size * step).astype(bf16)
            outs.append(pltpu.make_async_copy(cpy.at[f, t], whole.at[t], out_sem.at[f, t]))
            outs[-1].start()
        out[...] = dirb[f, z // 4, lax.rem(z, 4) * NY + y] * scale

    lax.fori_loop(1, NZ, wait_send(fz), 0)
    lax.fori_loop(1, NZ, wait_send(rz), 0)
    lax.fori_loop(1, NZ, wait_send(gz), 0)
    for copy in [*one, *two, swap, *ry, *gy, *sc, *yb]:
        copy.wait_send()
    for way in range(2):
        for s in range(1, HALF + 1):
            za(s, way).wait_send()
            zb(s, way).wait_send()
        for o in range(NZ):
            ya(o, way).wait_send()
            on(o, way).wait_send()
    for copy in outs:
        copy.wait()


def deliver(*refs):
    sem = refs[16]
    copies = [pltpu.make_async_copy(refs[i], refs[8 + i], sem.at[i]) for i in range(8)]
    for copy in copies:
        copy.start()
    for copy in copies:
        copy.wait()


def local(*args):
    vmem = pl.BlockSpec(memory_space=pltpu.VMEM)
    anywhere = pl.BlockSpec(memory_space=pl.ANY)
    dma = pltpu.SemaphoreType.DMA
    args = list(args)
    for k in (5, 6):
        args[k] = args[k].reshape(2, 16, 256)
    shapes = [jax.ShapeDtypeStruct((32, 256), f32)] * 2 + [jax.ShapeDtypeStruct((4, 256), f32)] * 4
    shapes += [jax.ShapeDtypeStruct((4, 16, 32, 256), bf16)] * 2
    out = pl.pallas_call(
        kernel,
        out_shape=tuple(shapes),
        in_specs=[anywhere] * 11,
        out_specs=(vmem,) * 6 + (anywhere,) * 2,
        scratch_shapes=[
            pltpu.VMEM((768, 2048), bf16),
            pltpu.VMEM((2, 768, 256), bf16),
            pltpu.VMEM((2, NZ, NY, 32, 256), f32),
            pltpu.VMEM((NZ, NY, 2, 16, 512), bf16),
            pltpu.VMEM((4, 4, 256), f32),
            pltpu.VMEM((2, 32, 8, 256), f32),
            pltpu.VMEM((NZ, NY, 8, 256), f32),
            pltpu.VMEM((NY - 1, NZ, 8, 256), f32),
            pltpu.VMEM((NZ, 8, 256), f32),
            pltpu.VMEM((NZ, 8, 256), f32),
            pltpu.VMEM((NZ, NY, 8, 256), f32),
            pltpu.VMEM((2, 4, 16, 32, 256), f32),
            pltpu.VMEM((NX * NC, 2, 8, 128), f32),
            pltpu.VMEM((2, 4, 16, 32, 256), bf16),
            dma((10,)),
            dma((NZ,)), dma((NZ,)),
            dma((2, 4)), dma((2, 4)), dma((2, 4)), dma((2, 4)),
            dma, dma,
            dma((NY,)), dma((NY,)), dma((NZ,)), dma((NZ,)),
            dma((NZ,)), dma((NZ,)), dma((NY,)), dma((NY,)),
            dma((NX * NC,)), dma((NX * NC,)),
            dma((2, HALF + 1)), dma((2, HALF + 1)), dma((2, HALF + 1)), dma((2, HALF + 1)),
            dma((4, NZ)), dma((4, NZ)), dma((NY,)), dma((NY,)),
            dma((2, 4)),
        ],
        compiler_params=pltpu.CompilerParams(
            collective_id=0, has_side_effects=True, vmem_limit_bytes=40 * 1024 * 1024
        ),
    )(*[pltpu.with_memory_space_constraint(a, pltpu.HBM) for a in args])
    out = pl.pallas_call(
        deliver,
        out_shape=tuple(shapes),
        in_specs=[anywhere] * 8,
        out_specs=(anywhere,) * 8,
        scratch_shapes=[dma((8,))],
        compiler_params=pltpu.CompilerParams(vmem_limit_bytes=1024 * 1024),
    )(*out)
    return (*out[:6], out[6].reshape(D, 256), out[7].reshape(D, 256))


def solution(mesh):
    finer = Mesh(mesh.devices.reshape(NZ, NY, NX, NC), ("fs_0", "fs_1", "tp_0", "tp_1"))
    rows, both = P(FS, None), P(FS, TP)
    return jax.shard_map(
        local,
        mesh=finer,
        in_specs=(rows, both, both, both, both, rows, rows, both, both, both, both),
        out_specs=(both,) * 6 + (P(None, TP),) * 2,
        check_vma=False,
    )
```

time: 137 us -> 89.7 us (0.65)
  the two profiles are of different devices: /device:TPU:16 before, /device:TPU:1 now
where the time goes in v2:
time: 89.7 us; the launch traced here: 88.8 us
  Pallas kernels  88.1 us (98%)
    pallas_call x1, Pallas kernels, local(): pl.pallas_call(kernel, out_shape=tuple(shapes), in_specs=[anywhere] * 11,...  86.7 us

profile of v2, /device:TPU:1, one launch (start us, length us, event | category | flops | bytes accessed | tf_op | source)
XLA Modules:
  0.0 88.8 jit_solution(12535186458999113093)
XLA Ops:
  0.6 86.7 %shard_map.170 = (f32[32,256]{1,0:T(8,128)S(1)}, f32[32,256]{1,0:T(8,128)S(1)}, f32[4,256]{1,0:T(4,128)S(1)}, f32[4,256]{1,0:T(4,128)S(1)}, f32[4,256]{1,0:T(4,1...) custom-call(bf16[768,2048]{1,0:T(8,128)(2,1)} %x_hbm.1, ...), custom_call_target="tpu_custom_call" | custom-call | tf_op jit(solution)/shard_map/pallas_call | solution.py:391
  87.3 1.4 %shard_map.171 = (f32[32,256]{1,0:T(8,128)}, f32[32,256]{1,0:T(8,128)}, f32[4,256]{1,0:T(4,128)}, f32[4,256]{1,0:T(4,128)}, f32[4,256]{1,0:T(4,128)}, /*index=5*...) custom-call(f32[32,256]{1,0:T(8,128)S(1)} %get-tuple-element.24.refs_0_, ...), custom_call_target="tpu_custom_call" | custom-call | tf_op jit(solution)/shard_map/pallas_call | solution.py:426

commit v3 on v2

--- a/solution.py
+++ b/solution.py
@@ -45,7 +45,7 @@
 def kernel(
     x_hbm, cin_hbm, cg_hbm, min_hbm, mg_hbm, fin_hbm, fg_hbm, a1_hbm, a2_hbm, g1_hbm, g2_hbm,
     step_in, step_g, o_a1, o_a2, o_g1, o_g2, copy_in, copy_g,
-    xb, cb, mf, fb, mom, lowt, lowb, rsy, l2, rsz, rb, dirb, sb, cpy,
+    xb, cb, gt, mf, fb, mom, res, lowb, rsy, l2, rsz, rb, dirb, sb, cpy,
     loc_sem, fz_s, fz_r, f1_s, f1_r, f2_s, f2_r, fc_s, fc_r,
     ry_s, ry_r, rz_s, rz_r, gz_s, gz_r, gy_s, gy_r, sc_s, sc_r,
     za_s, za_r, zb_s, zb_r, ya_s, ya_r, yb_s, yb_r, out_sem,
@@ -189,10 +189,23 @@
     ring_start(za)
     for copy in yb:
         copy.start()
+    for copy in loads[2:]:
+        copy.wait()
+
+    def gradient(f):
+        cot = cb[f].T
+        for t in range(4):
+            columns = pl.ds(t * 512, 512)
+            high, low = split_two(jnp.dot(cot, xb[:, columns], preferred_element_type=f32))
+            gt[f, pl.ds(0, 256), columns] = high
+            gt[f, pl.ds(256, 256), columns] = low
+
+    gradient(0)
     for copy in yb:
         copy.wait_recv()
     ring_start(zb)
     ring_next(za, 1)
+    gradient(1)
     ring_next(za, 2)
     lax.fori_loop(1, NZ, wait_recv(fz), 0)
 
@@ -220,106 +233,104 @@
     swap = remote(mine, mine, fc_s, fc_r, tp_1=other)
     swap.start()
     ring_next(za, 4)
-    for copy in loads[2:]:
-        copy.wait()
+    top = lax.broadcasted_iota(jnp.int32, (32, 8, 128), 1) < 4
+    pair = (c, other)
 
     def project(f):
-        total = jnp.zeros((256, 256), f32)
         factor = fb[:, :, :, :, pl.ds(pl.multiple_of(f * 256, 256), 256)].reshape(D, 256)
-        for t in range(3):
-            rows = pl.ds(t * 256, 256)
-            proj = jnp.dot(xb[rows, :], factor, preferred_element_type=f32)
-            high, low = split_two(proj.T)
-            cot = cb[f, rows, :]
-            total = total + jnp.dot(high, cot, preferred_element_type=f32)
-            total = total + jnp.dot(low, cot, preferred_element_type=f32)
-        lowt[f] = total.reshape(32, 8, 256)
+        both = jnp.dot(gt[f], factor, preferred_element_type=f32)
+        low = (both[:256] + both[256:]).T.reshape(32, 8, 256)
+        left, right = low[:, :, :128], low[:, :, 128:]
+        even = jnp.where(top, left, pltpu.roll(right, 4, 1)).reshape(16, 2, 8, 128)
+        odd = jnp.where(top, pltpu.roll(left, 4, 1), right).reshape(16, 2, 8, 128)
+        for k in range(2):
+            lowb[f, :, 2 * k] = even[:, k]
+            lowb[f, :, 2 * k + 1] = odd[:, k]
+
+    def sum_y(j):
+        copies = [
+            remote(lowb.at[pair[j], :, yy(k)], rsy.at[j, k - 1], ry_s.at[j, k], ry_r.at[j, k], fs_1=yy(k))
+            for k in range(1, NY)
+        ]
+        for copy in copies:
+            copy.start()
+        return copies
+
+    def rz(j):
+        return lambda k: remote(l2.at[j, zz(k)], rsz.at[j, k], rz_s.at[j, k], rz_r.at[j, k], fs_0=zz(k))
+
+    def gz(j):
+        part = rb.at[j, z, y]
+        return lambda k: remote(part, part, gz_s.at[j, k], gz_r.at[j, k], fs_0=zz(k))
 
     project(c)
+    ry = [sum_y(0)]
     ring_next(zb, 3)
     ring_next(za, 5)
     swap.wait_recv()
     project(other)
-    top = lax.broadcasted_iota(jnp.int32, (32, 8, 256), 1) < 4
-    low_a, low_b = lowt[0], lowt[1]
-    even = jnp.where(top, low_a, pltpu.roll(low_b, 4, 1))
-    odd = jnp.where(top, pltpu.roll(low_a, 4, 1), low_b)
-    for k in range(2):
-        lowb[:, 2 * k] = even.reshape(16, 2, 8, 256)[:, k]
-        lowb[:, 2 * k + 1] = odd.reshape(16, 2, 8, 256)[:, k]
-
-    ry = [
-        remote(lowb.at[:, yy(k)], rsy.at[k - 1], ry_s.at[k], ry_r.at[k], fs_1=yy(k))
-        for k in range(1, NY)
-    ]
-    for copy in ry:
-        copy.start()
+    ry.append(sum_y(1))
     ring_next(zb, 4)
     ring_next(za, 6)
-    acc = lowb[:, y]
-    for k, copy in enumerate(ry):
-        copy.wait_recv()
-        acc = acc + rsy[k]
-    l2[...] = acc
-
-    def rz(k):
-        return remote(l2.at[zz(k)], rsz.at[k], rz_s.at[k], rz_r.at[k], fs_0=zz(k))
-
-    lax.fori_loop(1, NZ, start(rz), 0)
+    for j in range(2):
+        acc = lowb[pair[j], :, y]
+        for k, copy in enumerate(ry[j]):
+            copy.wait_recv()
+            acc = acc + rsy[j, k]
+        l2[j] = acc
+        lax.fori_loop(1, NZ, start(rz(j)), 0)
     early = [0, *(o for s in range(1, HALF - 1) for o in (s, NZ - s))]
     late = [HALF - 1, HALF + 1, HALF]
     send_y(early)
     ring_next(zb, 5)
 
-    def add_one(k, total):
-        rz(k).wait_recv()
-        return total + rsz[k]
-
-    low = lax.fori_loop(1, NZ, add_one, l2[z])
-
-    first = jnp.concatenate([mom[0], mom[1]], axis=0)
-    second = jnp.concatenate([mom[2], mom[3]], axis=0)
-    first_new = first_decay * first + (1.0 - first_decay) * low
-    second_new = second_decay * second + (1.0 - second_decay) * low * low
-    rb[z, y] = first_new / (jnp.sqrt(second_new) + ratio_floor)
-
-    def gz(k):
-        part = rb.at[z, y]
-        return remote(part, part, gz_s.at[k], gz_r.at[k], fs_0=zz(k))
-
-    lax.fori_loop(1, NZ, start(gz), 0)
-    o_a1[...] = first_new[:4]
-    o_g1[...] = first_new[4:]
-    o_a2[...] = second_new[:4]
-    o_g2[...] = second_new[4:]
+    def folded(v):
+        return jnp.concatenate([v[:, :128], v[:, 128:]], axis=0)
+
+    def unfolded(v):
+        return jnp.concatenate([v[:4], v[4:]], axis=1)
+
+    for j in range(2):
+        def add_one(k, total, j=j):
+            rz(j)(k).wait_recv()
+            return total + rsz[j, k]
+
+        low = lax.fori_loop(1, NZ, add_one, l2[j, z])
+        first_new = first_decay * folded(mom[pair[j]]) + (1.0 - first_decay) * low
+        second_new = second_decay * folded(mom[2 + pair[j]]) + (1.0 - second_decay) * low * low
+        rb[j, z, y] = first_new / (jnp.sqrt(second_new) + ratio_floor)
+        lax.fori_loop(1, NZ, start(gz(j)), 0)
+        res[pair[j]] = unfolded(first_new)
+        res[2 + pair[j]] = unfolded(second_new)
     pass_y(early)
     ring_next(zb, 6)
-    lax.fori_loop(1, NZ, wait_recv(gz), 0)
-    gy = [
-        remote(rb.at[:, y], rb.at[:, y], gy_s.at[k], gy_r.at[k], fs_1=yy(k))
-        for k in range(1, NY)
-    ]
-    for copy in gy:
-        copy.start()
+    gy = []
+    for j in range(2):
+        lax.fori_loop(1, NZ, wait_recv(gz(j)), 0)
+        part = rb.at[j, :, y]
+        gy.append([
+            remote(part, part, gy_s.at[j, k], gy_r.at[j, k], fs_1=yy(k)) for k in range(1, NY)
+        ])
+        for copy in gy[j]:
+            copy.start()
+    for k, out in enumerate((o_a1, o_g1, o_a2, o_g2)):
+        out[...] = res[k]
     ring_next(za, 7)
     ring_next(zb, 7)
-    for copy in gy:
-        copy.wait_recv()
     ring_next(za, HALF)
     send_y(late)
-
-    ratio = rb[...].reshape(32, 2, 8, 256)
-    even, odd = ratio[:, 0], ratio[:, 1]
-    pieces = (
-        jnp.where(top, even, pltpu.roll(odd, 4, 1)).reshape(256, 256),
-        jnp.where(top, pltpu.roll(even, 4, 1), odd).reshape(256, 256),
-    )
-    for f in range(2):
-        high, lo = split_two(pieces[f])
-
+    for j in range(2):
+        f = pair[j]
+        for copy in gy[j]:
+            copy.wait_recv()
+        ratio = rb[j].reshape(32, 2, 8, 128)
+        even, odd = ratio[:, 0], ratio[:, 1]
+        left = jnp.where(top, even, pltpu.roll(odd, 4, 1)).reshape(256, 128)
+        right = jnp.where(top, pltpu.roll(even, 4, 1), odd).reshape(256, 128)
+        high, lo = split_two(jnp.concatenate([left, right], axis=1))
         acc = jnp.zeros((8, 256), f32)
         for t in range(4):
-            block = fb[4 * t:4 * t + 4, :, :, :, f * 256:(f + 1) * 256].reshape(512, 256)
+            block = fb[4 * t:4 * t + 4, :, :, :, pl.ds(pl.multiple_of(f * 256, 256), 256)].reshape(512, 256)
             d = jnp.dot(block, high, preferred_element_type=f32)
             d = d + jnp.dot(block, lo, preferred_element_type=f32)
             dirb[f, t] = d.reshape(16, 32, 256)
@@ -355,9 +366,10 @@
         out[...] = dirb[f, z // 4, lax.rem(z, 4) * NY + y] * scale
 
     lax.fori_loop(1, NZ, wait_send(fz), 0)
-    lax.fori_loop(1, NZ, wait_send(rz), 0)
-    lax.fori_loop(1, NZ, wait_send(gz), 0)
-    for copy in [*one, *two, swap, *ry, *gy, *sc, *yb]:
+    for j in range(2):
+        lax.fori_loop(1, NZ, wait_send(rz(j)), 0)
+        lax.fori_loop(1, NZ, wait_send(gz(j)), 0)
+    for copy in [*one, *two, swap, *ry[0], *ry[1], *gy[0], *gy[1], *sc, *yb]:
         copy.wait_send()
     for way in range(2):
         for s in range(1, HALF + 1):
@@ -396,15 +408,16 @@
         scratch_shapes=[
             pltpu.VMEM((768, 2048), bf16),
             pltpu.VMEM((2, 768, 256), bf16),
+            pltpu.VMEM((2, 512, 2048), bf16),
             pltpu.VMEM((2, NZ, NY, 32, 256), f32),
             pltpu.VMEM((NZ, NY, 2, 16, 512), bf16),
             pltpu.VMEM((4, 4, 256), f32),
-            pltpu.VMEM((2, 32, 8, 256), f32),
-            pltpu.VMEM((NZ, NY, 8, 256), f32),
-            pltpu.VMEM((NY - 1, NZ, 8, 256), f32),
-            pltpu.VMEM((NZ, 8, 256), f32),
-            pltpu.VMEM((NZ, 8, 256), f32),
-            pltpu.VMEM((NZ, NY, 8, 256), f32),
+            pltpu.VMEM((4, 4, 256), f32),
+            pltpu.VMEM((2, NZ, NY, 8, 128), f32),
+            pltpu.VMEM((2, NY - 1, NZ, 8, 128), f32),
+            pltpu.VMEM((2, NZ, 8, 128), f32),
+            pltpu.VMEM((2, NZ, 8, 128), f32),
+            pltpu.VMEM((2, NZ, NY, 8, 128), f32),
             pltpu.VMEM((2, 4, 16, 32, 256), f32),
             pltpu.VMEM((NX * NC, 2, 8, 128), f32),
             pltpu.VMEM((2, 4, 16, 32, 256), bf16),
@@ -412,8 +425,8 @@
             dma((NZ,)), dma((NZ,)),
             dma((2, 4)), dma((2, 4)), dma((2, 4)), dma((2, 4)),
             dma, dma,
-            dma((NY,)), dma((NY,)), dma((NZ,)), dma((NZ,)),
-            dma((NZ,)), dma((NZ,)), dma((NY,)), dma((NY,)),
+            dma((2, NY)), dma((2, NY)), dma((2, NZ)), dma((2, NZ)),
+            dma((2, NZ)), dma((2, NZ)), dma((2, NY)), dma((2, NY)),
             dma((NX * NC,)), dma((NX * NC,)),
             dma((2, HALF + 1)), dma((2, HALF + 1)), dma((2, HALF + 1)), dma((2, HALF + 1)),
             dma((4, NZ)), dma((4, NZ)), dma((NY,)), dma((NY,)),

time: 89.7 us -> 87.5 us (0.975)
  Pallas kernels: 88.1 us -> 86.7 us
    pallas_call x1, Pallas kernels: 86.7 us -> 85.3 us  [local(): pl.pallas_call(kernel, out_shape=tuple(shapes), in_specs=[anywhere] * 11,...]
where the time goes in v3:
time: 87.5 us; the launch traced here: 87.4 us
  Pallas kernels  86.7 us (99%)
    pallas_call x1, Pallas kernels, local(): pl.pallas_call(kernel, out_shape=tuple(shapes), in_specs=[anywhere] * 11,...  85.3 us

profile of v3, /device:TPU:1, one launch (start us, length us, event | category | flops | bytes accessed | tf_op | source)
XLA Modules:
  0.0 87.4 jit_solution(7581252605164950013)
XLA Ops:
  0.6 85.3 %shard_map.170 = (f32[32,256]{1,0:T(8,128)S(1)}, f32[32,256]{1,0:T(8,128)S(1)}, f32[4,256]{1,0:T(4,128)S(1)}, f32[4,256]{1,0:T(4,128)S(1)}, f32[4,256]{1,0:T(4,1...) custom-call(bf16[768,2048]{1,0:T(8,128)(2,1)} %x_hbm.1, ...), custom_call_target="tpu_custom_call" | custom-call | tf_op jit(solution)/shard_map/pallas_call | solution.py:403
  86.0 1.4 %shard_map.171 = (f32[32,256]{1,0:T(8,128)}, f32[32,256]{1,0:T(8,128)}, f32[4,256]{1,0:T(4,128)}, f32[4,256]{1,0:T(4,128)}, f32[4,256]{1,0:T(4,128)}, /*index=5*...) custom-call(f32[32,256]{1,0:T(8,128)S(1)} %get-tuple-element.24.refs_0_, ...), custom_call_target="tpu_custom_call" | custom-call | tf_op jit(solution)/shard_map/pallas_call | solution.py:439

commit v4 on v3

--- a/solution.py
+++ b/solution.py
@@ -71,7 +71,9 @@
         pl.semaphore_signal(barrier, inc=1, device_id={"fs_0": zz(k)}, device_id_type=pl.DeviceIdType.MESH)
         return 0
 
-    lax.fori_loop(1, NZ, greet, 0)
+    near = NZ // 4
+    lax.fori_loop(1, near + 1, greet, 0)
+    lax.fori_loop(NZ - near, NZ, greet, 0)
     for k in range(1, NY):
         pl.semaphore_signal(barrier, inc=1, device_id={"fs_1": yy(k)}, device_id_type=pl.DeviceIdType.MESH)
     tp_peers = [(dx, dc) for dx in range(NX) for dc in range(NC) if (dx, dc) != (0, 0)]
@@ -114,7 +116,7 @@
     own_tile(fin_hbm).wait()
     for copy in loads[:2]:
         copy.wait()
-    pl.semaphore_wait(barrier, NZ - 1 + NY - 1 + len(tp_peers))
+    pl.semaphore_wait(barrier, 2 * near + NY - 1 + len(tp_peers))
 
     def step_of(s, way):
         return (zz(1 - s), zz(1)) if way == 0 else (zz(s - 1), zz(-1))
@@ -163,9 +165,21 @@
         for k in range(1, NY)
     ]
 
-    def fz(k):
-        part = fb.at[z, y, h, :, tile]
-        return remote(part, part, fz_s.at[k], fz_r.at[k], fs_0=zz(k))
+    def fz(k, block=None, to=None):
+        part = fb.at[z if block is None else block, y, h, :, tile]
+        return remote(part, part, fz_s.at[k], fz_r.at[k], fs_0=zz(k) if to is None else to)
+
+    def relay():
+        passed = []
+        for j in range(1, near + 1):
+            fz(j).wait_recv()
+            passed.append(fz(near + j, zz(-j), zz(near)))
+            passed[-1].start()
+            fz(NZ - j).wait_recv()
+            if j < near:
+                passed.append(fz(NZ - near - j, zz(j), zz(-near)))
+                passed[-1].start()
+        return passed
 
     def start(make):
         def body(k, _):
@@ -185,7 +199,9 @@
             return 0
         return body
 
-    lax.fori_loop(1, NZ, start(fz), 0)
+    for j in range(1, near + 1):
+        fz(j).start()
+        fz(NZ - j).start()
     ring_start(za)
     for copy in yb:
         copy.start()
@@ -201,13 +217,18 @@
             gt[f, pl.ds(256, 256), columns] = low
 
     gradient(0)
+    passed = relay()
     for copy in yb:
         copy.wait_recv()
     ring_start(zb)
     ring_next(za, 1)
+    send_y([0, 1, NZ - 1])
     gradient(1)
     ring_next(za, 2)
-    lax.fori_loop(1, NZ, wait_recv(fz), 0)
+    send_y([2, NZ - 2])
+    ring_next(zb, 1)
+    for k in range(near + 1, NZ - near):
+        fz(k).wait_recv()
 
     def half_step(part_x, part_y, send, recv):
         copies = []
@@ -221,18 +242,19 @@
 
     lo_z, hi_z = pl.ds(0, HALF), pl.ds(HALF, HALF)
     one = half_step(fb.at[lo_z, y, h, :, tile], fb.at[hi_z, y, h, :, tile], f1_s, f1_r)
-    ring_next(zb, 1)
+    ring_next(za, 3)
     for copy in one:
         copy.wait_recv()
     two = half_step(fb.at[hi_z, :, h, :, tile], fb.at[lo_z, y, :, :, wide], f2_s, f2_r)
-    ring_next(za, 3)
     ring_next(zb, 2)
+    ring_next(za, 4)
     for copy in two:
         copy.wait_recv()
     mine = fb.at[:, :, :, :, wide]
     swap = remote(mine, mine, fc_s, fc_r, tp_1=other)
     swap.start()
-    ring_next(za, 4)
+    ring_next(zb, 3)
+    pass_y([0, 1, NZ - 1, 2, NZ - 2])
     top = lax.broadcasted_iota(jnp.int32, (32, 8, 128), 1) < 4
     pair = (c, other)
 
@@ -265,7 +287,6 @@
 
     project(c)
     ry = [sum_y(0)]
-    ring_next(zb, 3)
     ring_next(za, 5)
     swap.wait_recv()
     project(other)
@@ -279,7 +300,7 @@
             acc = acc + rsy[j, k]
         l2[j] = acc
         lax.fori_loop(1, NZ, start(rz(j)), 0)
-    early = [0, *(o for s in range(1, HALF - 1) for o in (s, NZ - s))]
+    early = [o for s in range(3, HALF - 1) for o in (s, NZ - s)]
     late = [HALF - 1, HALF + 1, HALF]
     send_y(early)
     ring_next(zb, 5)
@@ -303,7 +324,6 @@
         res[pair[j]] = unfolded(first_new)
         res[2 + pair[j]] = unfolded(second_new)
     pass_y(early)
-    ring_next(zb, 6)
     gy = []
     for j in range(2):
         lax.fori_loop(1, NZ, wait_recv(gz(j)), 0)
@@ -315,10 +335,11 @@
             copy.start()
     for k, out in enumerate((o_a1, o_g1, o_a2, o_g2)):
         out[...] = res[k]
+    ring_next(zb, 6)
     ring_next(za, 7)
-    ring_next(zb, 7)
     ring_next(za, HALF)
     send_y(late)
+    ring_next(zb, 7)
     for j in range(2):
         f = pair[j]
         for copy in gy[j]:
@@ -348,7 +369,7 @@
         copy.start()
     pass_y(late)
     ring_next(zb, HALF)
-    for o in [*early, *late]:
+    for o in range(NZ):
         for way in range(2):
             on(o, way).wait_recv()
     for copy in sc:
@@ -365,7 +386,8 @@
             outs[-1].start()
         out[...] = dirb[f, z // 4, lax.rem(z, 4) * NY + y] * scale
 
-    lax.fori_loop(1, NZ, wait_send(fz), 0)
+    for k in range(1, NZ):
+        fz(k).wait_send()
     for j in range(2):
         lax.fori_loop(1, NZ, wait_send(rz(j)), 0)
         lax.fori_loop(1, NZ, wait_send(gz(j)), 0)

time: 87.5 us -> 82.4 us (0.942)
  Pallas kernels: 86.7 us -> 81.5 us
    pallas_call x1, Pallas kernels: 85.3 us -> 80 us  [local(): pl.pallas_call(kernel, out_shape=tuple(shapes), in_specs=[anywhere] * 11,...]
where the time goes in v4:
time: 82.4 us; the launch traced here: 82.1 us
  Pallas kernels  81.5 us (99%)
    pallas_call x1, Pallas kernels, local(): pl.pallas_call(kernel, out_shape=tuple(shapes), in_specs=[anywhere] * 11,...  80 us

profile of v4, /device:TPU:1, one launch (start us, length us, event | category | flops | bytes accessed | tf_op | source)
XLA Modules:
  0.0 82.1 jit_solution(13588398937847448254)
XLA Ops:
  0.6 80.0 %shard_map.170 = (f32[32,256]{1,0:T(8,128)S(1)}, f32[32,256]{1,0:T(8,128)S(1)}, f32[4,256]{1,0:T(4,128)S(1)}, f32[4,256]{1,0:T(4,128)S(1)}, f32[4,256]{1,0:T(4,1...) custom-call(bf16[768,2048]{1,0:T(8,128)(2,1)} %x_hbm.1, ...), custom_call_target="tpu_custom_call" | custom-call | tf_op jit(solution)/shard_map/pallas_call | solution.py:425
  80.7 1.4 %shard_map.171 = (f32[32,256]{1,0:T(8,128)}, f32[32,256]{1,0:T(8,128)}, f32[4,256]{1,0:T(4,128)}, f32[4,256]{1,0:T(4,128)}, f32[4,256]{1,0:T(4,128)}, /*index=5*...) custom-call(f32[32,256]{1,0:T(8,128)S(1)} %get-tuple-element.24.refs_0_, ...), custom_call_target="tpu_custom_call" | custom-call | tf_op jit(solution)/shard_map/pallas_call | solution.py:461

commit v5 on v4

--- a/solution.py
+++ b/solution.py
@@ -216,14 +216,12 @@
             gt[f, pl.ds(0, 256), columns] = high
             gt[f, pl.ds(256, 256), columns] = low
 
-    gradient(0)
     passed = relay()
     for copy in yb:
         copy.wait_recv()
     ring_start(zb)
     ring_next(za, 1)
     send_y([0, 1, NZ - 1])
-    gradient(1)
     ring_next(za, 2)
     send_y([2, NZ - 2])
     ring_next(zb, 1)
@@ -246,7 +244,9 @@
     for copy in one:
         copy.wait_recv()
     two = half_step(fb.at[hi_z, :, h, :, tile], fb.at[lo_z, y, :, :, wide], f2_s, f2_r)
+    gradient(0)
     ring_next(zb, 2)
+    gradient(1)
     ring_next(za, 4)
     for copy in two:
         copy.wait_recv()
@@ -339,7 +339,6 @@
     ring_next(za, 7)
     ring_next(za, HALF)
     send_y(late)
-    ring_next(zb, 7)
     for j in range(2):
         f = pair[j]
         for copy in gy[j]:
@@ -367,6 +366,7 @@
     ]
     for copy in sc:
         copy.start()
+    ring_next(zb, 7)
     pass_y(late)
     ring_next(zb, HALF)
     for o in range(NZ):

time: 82.4 us -> 82.4 us (level)
  no operation moved by 1% of the time
where the time goes in v5:
time: 82.4 us; the launch traced here: 81.9 us
  Pallas kernels  81.2 us (99%)
    pallas_call x1, Pallas kernels, local(): pl.pallas_call(kernel, out_shape=tuple(shapes), in_specs=[anywhere] * 11,...  79.8 us

profile of v5, /device:TPU:1, one launch (start us, length us, event | category | flops | bytes accessed | tf_op | source)
XLA Modules:
  0.0 81.9 jit_solution(11195012005151754680)
XLA Ops:
  0.6 79.8 %shard_map.170 = (f32[32,256]{1,0:T(8,128)S(1)}, f32[32,256]{1,0:T(8,128)S(1)}, f32[4,256]{1,0:T(4,128)S(1)}, f32[4,256]{1,0:T(4,128)S(1)}, f32[4,256]{1,0:T(4,1...) custom-call(bf16[768,2048]{1,0:T(8,128)(2,1)} %x_hbm.1, ...), custom_call_target="tpu_custom_call" | custom-call | tf_op jit(solution)/shard_map/pallas_call | solution.py:425
  80.5 1.4 %shard_map.171 = (f32[32,256]{1,0:T(8,128)}, f32[32,256]{1,0:T(8,128)}, f32[4,256]{1,0:T(4,128)}, f32[4,256]{1,0:T(4,128)}, f32[4,256]{1,0:T(4,128)}, /*index=5*...) custom-call(f32[32,256]{1,0:T(8,128)S(1)} %get-tuple-element.24.refs_0_, ...), custom_call_target="tpu_custom_call" | custom-call | tf_op jit(solution)/shard_map/pallas_call | solution.py:461
